TPU v7x, 32 devices: a whole 2x2x4 slice. The times are simulated.
32 devices in a mesh: grp: 2 (over x), ep: 8 (over z, y), tp: 2 (over core).
Axes of the slice: x: 2, y: 2, z: 4, core: 2. Of those that a mesh axis runs over, the one named last changes fastest.
Arguments:
- tokens: bfloat16 [512, 2048], P(('grp', 'ep'), 'tp'), parts along dimension 0, may hold values from -6 to 6
- routes: int32 [512, 4], P(('grp', 'ep')), parts along dimension 0, may hold values from 0 to 7, all different within a row; in each aligned block of 32 rows (0 to 31, 32 to 63, ...) at most 18 rows name the same one
- gate_logits: float32 [512, 4], P(('grp', 'ep')), parts along dimension 0, may hold values from -6 to 6
- norm_gain: float32 [2048], P('tp'), may hold values from 0.1 to 1.9
- norm_shift: float32 [2048], P('tp'), may hold values from -3 to 3
- gate_weight: bfloat16 [8, 2048, 1024], P('ep', None, 'tp'), may hold values from -0.5 to 0.5
- up_weight: bfloat16 [8, 2048, 1024], P('ep', None, 'tp'), may hold values from -0.5 to 0.5
- down_weight: bfloat16 [8, 1024, 2048], P('ep', 'tp'), may hold values from -0.0234375 to 0.0234375
Outputs:
- mixed: bfloat16 [512, 2048], P(('grp', 'ep'), 'tp'), parts along dimension 0
There are 2 independent parts, one for each index of `grp`. A program takes and returns all parts, laid end to end along the dimension named above; an argument that names none is the same for every part. Nothing has to cross between parts.
Inputs may be any that keep to these rules, and one draw needn't show every extreme that they name: `routes`: each row names 4 different experts. Within the 32 rows of one index of ep no expert is named more than 18 times, a bound that some blocks reach.
All inputs are finite; a program needn't handle non-finite values.
Results may differ from a plain program's by a relative error of at most 0.012.
Values may be sent and summed in bfloat16 or wider, within the bound.
A program may use at most 64 MiB of HBM per device.

v0:
```python
import jax
import jax.numpy as jnp
from jax import lax
from jax.sharding import PartitionSpec as P

norm_eps = 1e-05
clamp_limit = 7.0
sigmoid_slope = 1.702


def expert_apply(received, gate_weight, up_weight, down_weight):
    whole = lax.all_gather(received, "tp", axis=2, tiled=True)
    sources, slots_here, width = whole.shape
    row_block = whole.reshape(sources * slots_here, width)
    gate_pre = jnp.dot(row_block, gate_weight[0], preferred_element_type=jnp.float32)
    up_pre = jnp.dot(row_block, up_weight[0], preferred_element_type=jnp.float32)
    gate_cut = jnp.minimum(gate_pre, clamp_limit)
    up_cut = jnp.clip(up_pre, -clamp_limit, clamp_limit)
    hidden = ((up_cut + 1.0) * gate_cut * jax.nn.sigmoid(sigmoid_slope * gate_cut)).astype(
        jnp.bfloat16
    )
    partial_out = jnp.dot(hidden, down_weight[0], preferred_element_type=jnp.float32).astype(
        jnp.bfloat16
    )
    summed = lax.psum_scatter(
        partial_out.reshape(sources, slots_here, width), "tp", scatter_dimension=2, tiled=True
    ).astype(jnp.float32)
    return summed.astype(jnp.bfloat16)


def slot_ranks(flat_experts, expert_count):
    onehot = (flat_experts[:, None] == jnp.arange(expert_count, dtype=jnp.int32)[None, :]).astype(
        jnp.int32
    )
    earlier = jnp.cumsum(onehot, axis=0) - onehot
    return jnp.sum(earlier * onehot, axis=1)


def body(tokens, routes, gate_logits, norm_gain, norm_shift, gate_weight, up_weight, down_weight):
    ep_count = lax.axis_size("ep")
    tok_rows, top_count = routes.shape
    half_width = tokens.shape[1]
    full_width = half_width * lax.axis_size("tp")
    capacity = tok_rows * top_count // ep_count + 2
    floats = tokens.astype(jnp.float32)
    entire = lax.all_gather(tokens, "tp", axis=1, tiled=True).astype(jnp.float32)
    row_sums = jnp.sum(entire, axis=1)
    row_squares = jnp.sum(entire * entire, axis=1)
    average = row_sums / full_width
    variance = row_squares / full_width - average * average
    normed = (
        (floats - average[:, None]) * lax.rsqrt(variance[:, None] + norm_eps) * norm_gain
        + norm_shift
    ).astype(jnp.bfloat16)
    send_width = normed.shape[1]
    exp_logits = jnp.exp(gate_logits)
    weights = exp_logits / jnp.sum(exp_logits, axis=1, keepdims=True)
    flat_experts = routes.reshape(-1)
    slot_index = flat_experts * capacity + slot_ranks(flat_experts, ep_count)
    token_index = jnp.arange(tok_rows * top_count, dtype=jnp.int32) // top_count
    outgoing = (
        jnp.zeros((ep_count * capacity, send_width), jnp.bfloat16)
        .at[slot_index]
        .set(normed[token_index])
    )
    answered = expert_apply(
        lax.all_to_all(
            outgoing.reshape(ep_count, capacity, send_width),
            "ep",
            split_axis=0,
            concat_axis=0,
            tiled=True,
        ),
        gate_weight,
        up_weight,
        down_weight,
    )
    returned = lax.all_to_all(answered, "ep", split_axis=0, concat_axis=0, tiled=True)
    picked = returned.reshape(ep_count * capacity, half_width)[slot_index].astype(jnp.float32)
    mixed = jnp.sum(picked.reshape(tok_rows, top_count, half_width) * weights[:, :, None], axis=1)
    return mixed.astype(jnp.bfloat16)


def solution(mesh):
    placed = (
        P(("grp", "ep"), "tp"),
        P(("grp", "ep"), None),
        P(("grp", "ep"), None),
        P("tp"),
        P("tp"),
        P("ep", None, "tp"),
        P("ep", None, "tp"),
        P("ep", "tp", None),
    )
    return jax.shard_map(
        body, mesh=mesh, in_specs=placed, out_specs=P(("grp", "ep"), "tp"), check_vma=False
    )
```

profile of v0, /device:TPU:0, one launch (start us, length us, event | category | flops | bytes accessed | tf_op | source)
XLA Modules:
  0.0 76.7 jit_solution(17263235784279741785)
XLA Ops:
  6.5 0.0 copy-start
  6.5 0.0 reduce-scatter.2.cloned.1.call-start
  6.5 0.9 %copy.13 = s32[32,4]{1,0:T(8,128)S(1)} copy(s32[32,4]{0,1:T(4,128)} %param.9) | data formatting | bytes 1024 | tf_op args[1]
  7.5 0.7 broadcast_multiply_fusion
  8.1 2.2 %all_gather.6 = bf16[32,2048]{1,0:T(8,128)(2,1)S(1)} all-gather(bf16[32,1024]{1,0:T(8,128)(2,1)} %param.8), channel_id=1, replica_groups=mesh['grp'=2,'ep'=8,'tp'=2] {'tp'}, dimensions={1}, use_global_device_ids=true | all-gather | bytes 196608 | tf_op jit(solution)/shard_map/all_gather | solution.py:46
  10.4 0.1 convert_reduce_fusion
  10.5 0.1 eq.15
  10.6 0.1 fusion.38
  10.7 0.2 reduce_window_sum.11
  10.9 0.2 select_reduce_fusion
  11.1 0.1 copy.12
  11.2 0.1 mul.67
  11.3 0.9 %add_convert_fusion = bf16[32,1024]{1,0:T(8,128)(2,1)S(1)} fusion(bf16[32,1024]{1,0:T(8,128)(2,1)} %param.8, f32[1024]{0:T(1024)} %param.12, f32[1024]{0:T(1024)} %param.11, f32[32]{0:T(128)S(1)} %get-tuple-element.8, f32[32]{0:T(128)S(1)} %get-tuple-element.7), kind=kLoop, calls=%fused_computation.31 | loop fusion | flops 196608 | bytes 139520 | tf_op jit(solution)/shard_map/convert_element_type | solution.py:54
  12.3 2.1 %scatter_custom_fusion = bf16[144,1024]{1,0:T(8,128)(2,1)S(1)} fusion(s32[128]{0:T(128)S(1)} %fusion.40, bf16[32,1024]{1,0:T(8,128)(2,1)S(1)} %add_convert_fusion, s32[1024]{0:T(1024)S(1)} %pad_clamp_fusion.1, bf16[]{:T(256)} %constant.17.clone.1), kind=kCustom, calls=%fused_computation.24 | custom fusion | bytes 294914 | tf_op jit(solution)/shard_map/scatter | solution.py:64
  14.4 0.1 reshape.107
  14.5 19.3 %all_to_all.10 = bf16[8,18,1024]{2,1,0:T(8,128)(2,1)S(1)} all-to-all(bf16[8,18,1024]{2,1,0:T(8,128)(2,1)S(1)} %reshape.107), channel_id=1, replica_groups=mesh['grp'=2,'ep'=8,'tp'=2] {'ep'}, dimensions={0} | all-to-all | bytes 589824 | tf_op jit(solution)/shard_map/all_to_all | solution.py:67
  33.8 2.4 %all_gather.7 = bf16[8,18,2048]{2,1,0:T(8,128)(2,1)S(1)} all-gather(bf16[8,18,1024]{2,1,0:T(8,128)(2,1)S(1)} %all_to_all.10), channel_id=1, replica_groups=mesh['grp'=2,'ep'=8,'tp'=2] {'tp'}, dimensions={2}, use_global_device_ids=true | all-gather | bytes 884736 | tf_op jit(solution)/shard_map/all_gather | solution.py:12
  36.2 0.2 reshape.108
  36.4 2.8 %fusion.5 = f32[144,512]{1,0:T(8,128)} fusion(bf16[144,2048]{1,0:T(8,128)(2,1)S(1)} %reshape.108, bf16[1,2048,512]{2,1,0:T(8,128)(2,1)} %param.13), kind=kOutput, calls=%fused_computation.9 | convolution fusion | flops 302063616 | bytes 2981888 | tf_op jit(solution)/shard_map/dot_general | solution.py:15
  39.2 0.0 copy-done
  39.2 2.5 %convolution_convert_fusion = bf16[144,2048]{1,0:T(8,128)(2,1)S(1)} fusion(bf16[1,512,2048]{2,1,0:T(8,128)(2,1)S(1)} %copy-done, f32[144,512]{1,0:T(8,128)} %fusion.5, bf16[144,2048]{1,0:T(8,128)(2,1)S(1)} %reshape.108, bf16[1,2048,512]{2,1,0:T(8,128)(2,1)} %param.14), kind=kOutput, calls=%fused_computation.3 | convolution fusion | flops 604938240 | bytes 5668864 | tf_op jit(solution)/shard_map/dot_general | solution.py:22
  41.7 0.0 copy-start.1
  41.7 1.0 %reshape.109 = bf16[8,18,2048]{2,1,0:T(8,128)(2,1)} reshape(bf16[144,2048]{1,0:T(8,128)(2,1)S(1)} %convolution_convert_fusion) | data formatting | bytes 1179648 | tf_op jit(solution)/shard_map/reshape | solution.py:26
  42.8 0.0 reduce-scatter.2.cloned.1.call-update
  42.8 7.0 %reduce-scatter.2.cloned.1.call-done = bf16[8,18,1024]{2,1,0:T(8,128)(2,1)} async-done(((bf16[8,18,2048]{2,1,0:T(8,128)(2,1)}), bf16[8,18,1024]{2,1,0:T(8,128)(2,1)}) %reduce-scatter.2.cloned.1.call-update) | async-done | bytes 294928 | tf_op jit(solution)/shard_map/reduce_scatter | solution.py:25
  49.8 5.7 %all-to-all-start.1 = ((bf16[8,18,1024]{2,1,0:T(8,128)(2,1)}), bf16[8,18,1024]{2,1,0:T(8,128)(2,1)S(1)}, u32[]{:S(2)}, u32[]{:S(2)}) async-start(bf16[8,18,1024]{2,1,0:T(8,128)(2,1)} %reduce-scatter.2.cloned.1.call-done), calls=%async_computation.2 | async-start | bytes 786432 | tf_op jit(solution)/shard_map/all_to_all | solution.py:78
  55.5 0.0 copy-done.1
  55.5 0.1 copy.14
  55.6 12.0 %all-to-all-done.1 = bf16[8,18,1024]{2,1,0:T(8,128)(2,1)S(1)} async-done(((bf16[8,18,1024]{2,1,0:T(8,128)(2,1)}), bf16[8,18,1024]{2,1,0:T(8,128)(2,1)S(1)}, u32[]{:S(2)}, u32[]{:S(2)}) %all-to-all-start.1) | async-done | bytes 294944 | tf_op jit(solution)/shard_map/all_to_all | solution.py:78
  67.7 0.1 reshape.110
  67.8 0.9 %gather_fusion = bf16[128,1024]{1,0:T(8,128)(2,1)S(1)} fusion(bf16[144,1024]{1,0:T(8,128)(2,1)S(1)} %reshape.110, s32[1024]{0:T(1024)S(1)} %pad_clamp_fusion), kind=kCustom, calls=%fused_computation.1 | custom fusion | bytes 524800 | tf_op jit(solution)/shard_map/gather | solution.py:79
  68.6 0.2 reshape.111
  68.8 1.0 %multiply_reduce_fusion = bf16[32,1024]{1,0:T(8,128)(2,1)} fusion(f32[32,4,1024]{2,1,0:T(4,128)S(1)} %reshape.111, f32[32,4]{1,0:T(8,128)S(1)} %copy.14), kind=kLoop, calls=%fused_computation.15 | loop fusion | flops 229376 | bytes 590336 | tf_op jit(solution)/shard_map/reduce_sum | solution.py:80
  (7 shorter events, 0.1 us)
Async XLA Ops:
  6.5 32.6 %copy-start = (bf16[1,512,2048]{2,1,0:T(8,128)(2,1)S(1)}, bf16[1,512,2048]{2,1,0:T(8,128)(2,1)}, u32[]{:S(2)}) copy-start(bf16[1,512,2048]{2,1,0:T(8,128)(2,1)} %param.15) | copy-start | bytes 6291460
  6.5 43.2 %reduce-scatter.2.cloned.1.call-start = ((), (), s32[]{:S(2)}) async-start(), calls=%async_computation.3 | async-start | bytes 1179648 | tf_op jit(solution)/shard_map/reduce_scatter | solution.py:25
  41.7 13.8 %copy-start.1 = (f32[32,4]{0,1:T(4,128)S(1)}, f32[32,4]{0,1:T(4,128)}, u32[]{:S(2)}) copy-start(f32[32,4]{0,1:T(4,128)} %param.10) | copy-start | bytes 1540
  49.8 17.9 %all-to-all-start.1 = ((bf16[8,18,1024]{2,1,0:T(8,128)(2,1)}), bf16[8,18,1024]{2,1,0:T(8,128)(2,1)S(1)}, u32[]{:S(2)}, u32[]{:S(2)}) async-start(bf16[8,18,1024]{2,1,0:T(8,128)(2,1)} %reduce-scatter.2.cloned.1.call-done), calls=%async_computation.2 | async-start | bytes 786432 | tf_op jit(solution)/shard_map/all_to_all | solution.py:78
Sparse Core Ops, SparseCore 0:
  42.9 6.8 reduce-scatter.1
where the time goes:
time: 77.1 us; the launch traced here: 76.7 us
  blocking collectives  23.9 us (31%)
  waiting for transfers between devices  19.1 us (25%)
  between operations  13.5 us (18%)
  local copies, waits for them, and re-layouts  5.87 us (8%)
  starting transfers between devices  5.72 us (7%)
  matrix products  5.3 us (7%)
  other arithmetic  3.3 us (4%)
    all_to_all x1, blocking collectives, body(): lax.all_to_all(outgoing.reshape(ep_count, capacity, send_width), 'ep', sp...  19.3 us
    all_to_all x1, waiting for transfers between devices, body(): lax.all_to_all(answered, 'ep', split_axis=0, concat_axis=0, tiled=True)  12 us
    reduce_scatter x1, waiting for transfers between devices, expert_apply(): lax.psum_scatter(partial_out.reshape(sources, slots_here, width), 'tp', s...  7 us
    all_to_all x1, starting transfers between devices, body(): lax.all_to_all(answered, 'ep', split_axis=0, concat_axis=0, tiled=True)  5.72 us
    dot_general x1, matrix products, expert_apply(): jnp.dot(row_block, gate_weight[0], preferred_element_type=jnp.float32)  2.78 us
    dot_general x1, matrix products, expert_apply(): jnp.dot(hidden, down_weight[0], preferred_element_type=jnp.float32)  2.51 us
    all_gather x1, blocking collectives, expert_apply(): whole = lax.all_gather(received, 'tp', axis=2, tiled=True)  2.36 us
    all_gather x1, blocking collectives, body(): lax.all_gather(tokens, 'tp', axis=1, tiled=True).astype(jnp.float32)  2.25 us
  transfers between devices with their start and end apart: 2, of which 2 were waited for; matrix products, arithmetic and copies ran while one was open for 0% of the time, Pallas kernels for 0%

commit v1 on v0

v1 whole, which is shorter than its diff:
```python
import functools

import jax
import jax.numpy as jnp
from jax import lax
from jax.experimental import pallas as pl
from jax.experimental.pallas import tpu as pltpu
from jax.sharding import PartitionSpec as P

norm_eps = 1e-05
clamp_limit = 7.0
sigmoid_slope = 1.702
MESH = pl.DeviceIdType.MESH
f32 = jnp.float32
bf16 = jnp.bfloat16


def kernel(
    n, cap, pad,
    tokens_ref, routes_ref, logits_ref, gain_ref, shift_ref, wg_hbm, wu_hbm, wd_hbm,
    out_ref,
    wg, wu, wd, stat_out, stat_in, outb, rows, part_out, part_in, answer, back,
    w_sem, st_sem, d_send, d_recv, f_send, f_recv, p_send, p_recv, r_send, r_recv,
):
    me = lax.axis_index("ep")
    tp = lax.axis_index("tp")
    other = 1 - tp
    half = tokens_ref.shape[1]
    width = 2 * half
    toks, top = routes_ref.shape
    slots = n * pad
    paired = n & (n - 1) == 0

    def peer(d, sign):
        if not paired:
            return lax.rem(me + sign * d + n, n)
        where, bit = me, 1
        while bit < n:
            if d & bit:
                where = where + bit * (1 - 2 * lax.rem(me // bit, 2))
            bit *= 2
        return where

    order = list(range(n - 1, 0, -1))
    target = [me] + [peer(d, 1) for d in range(1, n)]
    source = [me] + [peer(d, -1) for d in range(1, n)]

    barrier = pltpu.get_barrier_semaphore()
    pl.semaphore_signal(barrier, inc=1, device_id={"tp": other}, device_id_type=MESH)
    for d in order:
        pl.semaphore_signal(barrier, inc=1, device_id={"ep": target[d]}, device_id_type=MESH)
    loads = [
        pltpu.make_async_copy(wg_hbm.at[0], wg, w_sem.at[0]),
        pltpu.make_async_copy(wu_hbm.at[0], wu, w_sem.at[1]),
        pltpu.make_async_copy(wd_hbm.at[0], wd, w_sem.at[2]),
    ]
    for load in loads:
        load.start()

    x = tokens_ref[...].astype(f32)
    sum_one = jnp.sum(x, axis=1, keepdims=True)
    sum_two = jnp.sum(x * x, axis=1, keepdims=True)
    lane = lax.broadcasted_iota(jnp.int32, (toks, 128), 1)
    stat_out[...] = jnp.where(lane == 0, sum_one, sum_two)

    column = lax.broadcasted_iota(jnp.int32, (toks, slots), 1)
    expert, rank = column // pad, column % pad
    logits = jnp.exp(logits_ref[...])
    weights = logits / jnp.sum(logits, axis=1, keepdims=True)
    routes = routes_ref[...]
    named = jnp.zeros((toks, slots), f32)
    share = jnp.zeros((toks, slots), f32)
    for k in range(top):
        hit = routes[:, k:k + 1] == expert
        named = jnp.where(hit, 1.0, named)
        share = jnp.where(hit, weights[:, k:k + 1], share)
    earlier = (
        lax.broadcasted_iota(jnp.int32, (toks, toks), 1)
        < lax.broadcasted_iota(jnp.int32, (toks, toks), 0)
    )
    ranks = jnp.dot(
        jnp.where(earlier, 1.0, 0.0).astype(bf16), named.astype(bf16), preferred_element_type=f32
    )
    chosen = (named > 0.5) & (ranks == rank.astype(f32))
    share = jnp.where(chosen, share, 0.0)
    pick = jnp.transpose(jnp.where(chosen, 1.0, 0.0)).astype(bf16)
    share_a = share.astype(bf16)
    rest = share - share_a.astype(f32)
    share_b = rest.astype(bf16)
    share_c = (rest - share_b.astype(f32)).astype(bf16)

    back[...] = jnp.zeros_like(back)
    pl.semaphore_wait(barrier, n)

    stat = pltpu.make_async_remote_copy(
        stat_out, stat_in, st_sem.at[0], st_sem.at[1], device_id={"tp": other}, device_id_type=MESH
    )
    stat.start()
    stat.wait()
    average = (sum_one + stat_in[:, 0:1]) / width
    variance = (sum_two + stat_in[:, 1:2]) / width - average * average
    normed = (
        (x - average) * lax.rsqrt(variance + norm_eps) * gain_ref[...] + shift_ref[...]
    ).astype(bf16)
    outb[...] = jnp.dot(pick, normed, preferred_element_type=f32).astype(bf16).reshape(n, pad, half)

    def dispatch(d):
        return pltpu.make_async_remote_copy(
            outb.at[target[d], pl.ds(0, cap)], rows.at[tp, me, pl.ds(0, cap)],
            d_send.at[d], d_recv.at[d], device_id={"ep": target[d]}, device_id_type=MESH,
        )

    def forward(d):
        spot = rows.at[tp, source[d], pl.ds(0, cap)]
        return pltpu.make_async_remote_copy(
            spot, spot, f_send.at[d], f_recv.at[d], device_id={"tp": other}, device_id_type=MESH
        )

    for d in order:
        dispatch(d).start()
    rows[tp, me] = outb[me]
    forward(0).start()
    for d in reversed(order):
        dispatch(d).wait_recv()
        forward(d).start()
    for load in loads:
        load.wait()
    for d in range(n):
        forward(d).wait_recv()

    ff = wg.shape[1]
    left = rows[0].reshape(slots, half)
    right = rows[1].reshape(slots, half)
    gate = jnp.dot(left, wg[:half], preferred_element_type=f32) + jnp.dot(
        right, wg[half:], preferred_element_type=f32
    )
    up = jnp.dot(left, wu[:half], preferred_element_type=f32) + jnp.dot(
        right, wu[half:], preferred_element_type=f32
    )
    cut = jnp.minimum(gate, clamp_limit)
    hidden = (
        (jnp.clip(up, -clamp_limit, clamp_limit) + 1.0) * cut * jax.nn.sigmoid(sigmoid_slope * cut)
    ).astype(bf16)

    def columns(index):
        return pl.ds(pl.multiple_of(index * half, half), half)

    part_out[...] = (
        jnp.dot(hidden, wd[:, columns(other)], preferred_element_type=f32)
        .astype(bf16).reshape(n, pad, half)
    )

    def partial(d):
        return pltpu.make_async_remote_copy(
            part_out.at[source[d], pl.ds(0, cap)], part_in.at[source[d], pl.ds(0, cap)],
            p_send.at[d], p_recv.at[d], device_id={"tp": other}, device_id_type=MESH,
        )

    def give_back(d):
        return pltpu.make_async_remote_copy(
            answer.at[source[d], pl.ds(0, cap)], back.at[me, pl.ds(0, cap)],
            r_send.at[d], r_recv.at[d], device_id={"ep": source[d]}, device_id_type=MESH,
        )

    for d in order + [0]:
        partial(d).start()
    answer[...] = (
        jnp.dot(hidden, wd[:, columns(tp)], preferred_element_type=f32)
        .astype(bf16).reshape(n, pad, half)
    )
    for d in order + [0]:
        partial(d).wait_recv()
        spot = source[d]
        total = (
            answer[spot, pl.ds(0, cap)].astype(f32) + part_in[spot, pl.ds(0, cap)].astype(f32)
        ).astype(bf16)
        if d:
            answer[spot, pl.ds(0, cap)] = total
            give_back(d).start()
        else:
            back[me, pl.ds(0, cap)] = total
    for d in reversed(order):
        give_back(d).wait_recv()
    got = back[...].reshape(slots, half)
    mixed = (
        jnp.dot(share_c, got, preferred_element_type=f32)
        + jnp.dot(share_b, got, preferred_element_type=f32)
        + jnp.dot(share_a, got, preferred_element_type=f32)
    )
    out_ref[...] = mixed.astype(bf16)
    for d in range(n):
        forward(d).wait_send()
        partial(d).wait_send()
        if d:
            dispatch(d).wait_send()
            give_back(d).wait_send()


def body(tokens, routes, gate_logits, norm_gain, norm_shift, gate_weight, up_weight, down_weight):
    n = lax.axis_size("ep")
    toks, top = routes.shape
    half = tokens.shape[1]
    cap = toks * top // n + 2
    pad = -(-cap // 16) * 16
    cap = -(-cap // 8) * 8
    ff = gate_weight.shape[2]
    vmem = pl.BlockSpec(memory_space=pltpu.VMEM)
    hbm = pl.BlockSpec(memory_space=pl.ANY)
    block = pltpu.VMEM((n, pad, half), bf16)
    sems = pltpu.SemaphoreType.DMA((n,))
    return pl.pallas_call(
        functools.partial(kernel, n, cap, pad),
        out_shape=jax.ShapeDtypeStruct((toks, half), bf16),
        in_specs=[vmem] * 5 + [hbm] * 3,
        out_specs=vmem,
        scratch_shapes=[
            pltpu.VMEM((2 * half, ff), bf16),
            pltpu.VMEM((2 * half, ff), bf16),
            pltpu.VMEM((ff, 2 * half), bf16),
            pltpu.VMEM((toks, 128), f32),
            pltpu.VMEM((toks, 128), f32),
            block,
            pltpu.VMEM((2, n, pad, half), bf16),
            block, block, block, block,
            pltpu.SemaphoreType.DMA((3,)),
            pltpu.SemaphoreType.DMA((2,)),
            sems, sems, sems, sems, sems, sems, sems, sems,
        ],
        compiler_params=pltpu.CompilerParams(collective_id=0, has_side_effects=True),
    )(
        tokens, routes, gate_logits, norm_gain.reshape(1, half), norm_shift.reshape(1, half),
        gate_weight, up_weight, down_weight,
    )


def solution(mesh):
    placed = (
        P(("grp", "ep"), "tp"),
        P(("grp", "ep"), None),
        P(("grp", "ep"), None),
        P("tp"),
        P("tp"),
        P("ep", None, "tp"),
        P("ep", None, "tp"),
        P("ep", "tp", None),
    )
    return jax.shard_map(
        body, mesh=mesh, in_specs=placed, out_specs=P(("grp", "ep"), "tp"), check_vma=False
    )
```

time: 77.1 us -> 36.9 us (0.48)
  Pallas kernels: 0 us -> 32.4 us
  blocking collectives: 23.9 us -> 0 us
  waiting for transfers between devices: 19.1 us -> 0 us
  between operations: 13.5 us -> 0.01 us
  starting transfers between devices: 5.72 us -> 0 us
  matrix products: 5.3 us -> 0 us
  other arithmetic: 3.3 us -> 0 us
  local copies, waits for them, and re-layouts: 5.87 us -> 4.2 us
    pallas_call x0 -> x1, Pallas kernels: none -> 32.4 us  [body(): pl.pallas_call(functools.partial(kernel, n, cap, pad), out_shape=jax.Shap...]
    all_to_all x1 -> x0, blocking collectives: 19.3 us -> none  [body(): lax.all_to_all(outgoing.reshape(ep_count, capacity, send_width), 'ep', sp...]
    all_to_all x1 -> x0, waiting for transfers between devices: 12 us -> none  [body(): lax.all_to_all(answered, 'ep', split_axis=0, concat_axis=0, tiled=True)]
    reduce_scatter x1 -> x0, waiting for transfers between devices: 7 us -> none  [expert_apply(): lax.psum_scatter(partial_out.reshape(sources, slots_here, width), 'tp', s...]
    all_to_all x1 -> x0, starting transfers between devices: 5.72 us -> none  [body(): lax.all_to_all(answered, 'ep', split_axis=0, concat_axis=0, tiled=True)]
    dot_general x2 -> x0, matrix products: 5.3 us -> none  [the longest x1 2.78 us: expert_apply(): jnp.dot(row_block, gate_weight[0], preferred_element_type=jnp.float32)]
    all_gather x2 -> x0, blocking collectives: 4.61 us -> none  [the longest x1 2.36 us: expert_apply(): whole = lax.all_gather(received, 'tp', axis=2, tiled=True)]
    unnamed x5 -> x3, local copies, waits for them, and re-layouts: 0.92 us -> 4.2 us
  transfers between devices with their start and end apart: 2 -> 0, of which waited for: 2 -> 0; matrix products, arithmetic and copies ran while one was open for 0% -> 0% of each run, Pallas kernels for 0% -> 0%
where the time goes in v1:
time: 36.9 us; the launch traced here: 36.6 us
  Pallas kernels  32.4 us (88%)
  local copies, waits for them, and re-layouts  4.2 us (11%)
    pallas_call x1, Pallas kernels, body(): pl.pallas_call(functools.partial(kernel, n, cap, pad), out_shape=jax.Shap...  32.4 us
    unnamed x3, local copies, waits for them, and re-layouts  4.2 us

profile of v1, /device:TPU:0, one launch (start us, length us, event | category | flops | bytes accessed | tf_op | source)
XLA Modules:
  0.0 36.6 jit_solution(7335553923877825932)
XLA Ops:
  0.0 1.4 %copy.9.routes_ref = s32[32,4]{1,0:T(8,128)} copy(s32[32,4]{0,1:T(4,128)} %param.9) | data formatting | bytes 1024 | tf_op args[1]
  1.4 1.4 %copy.10.logits_ref = f32[32,4]{1,0:T(8,128)} copy(f32[32,4]{0,1:T(4,128)} %param.10) | data formatting | bytes 1024 | tf_op args[2]
  2.7 32.4 %shard_map.82 = bf16[32,1024]{1,0:T(8,128)(2,1)} custom-call(bf16[32,1024]{1,0:T(8,128)(2,1)} %tokens_ref.1, s32[32,4]{1,0:T(8,128)} %copy.9.routes_ref, f32[32,4]{1,0:T(8,128)} %copy.10.logits_ref, f32[1,1024]{1,0:T(1,128)} %bitcast.2, f32[1,1024]{1,0:T(1,128)} %bitcast.3, bf16[1,2048,512]{2,1,0:T(8,128)(2,1)} %wg_hbm.1, bf16[1,2048,512]{2,1,0:T(8,128)(2,1)} %wu_hbm.1, ...), custom_call_target="tpu_custom_call" | custom-call | tf_op jit(solution)/shard_map/pallas_call | solution.py:211
  35.2 1.5 %copy.12 = bf16[32,1024]{1,0:T(8,128)(2,1)} copy(bf16[32,1024]{1,0:T(8,128)(2,1)} %shard_map.82) | data formatting | bytes 131072

commit v2 on v0

v2 whole, which is shorter than its diff:
```python
import functools

import jax
import jax.numpy as jnp
from jax import lax
from jax.experimental import pallas as pl
from jax.experimental.pallas import tpu as pltpu
from jax.sharding import PartitionSpec as P

norm_eps = 1e-05
clamp_limit = 7.0
sigmoid_slope = 1.702
MESH = pl.DeviceIdType.MESH
LANES = 128
f32 = jnp.float32
bf16 = jnp.bfloat16


def dot(a, b):
    return jnp.dot(a, b, preferred_element_type=f32)


def iota(shape, axis):
    return lax.broadcasted_iota(jnp.int32, shape, axis)


def kernel(
    n, base, rem, seq, groups, sends,
    tokens_hbm, routes_hbm, logits_hbm, gain_hbm, shift_hbm, wg_hbm, wu_hbm, wd_hbm,
    out_ref,
    tok, routes_ref, logits_ref, affine, wg, wu, wd,
    outb1, outb2, rows1, rows2, part_out, part_in, ans1, ans2, back1, back2,
    i_sem, w_sem, a_sem, d_send, d_recv, f_send, f_recv, p_send, p_recv, r_send, r_recv,
):
    me = lax.axis_index("ep")
    tp = lax.axis_index("tp")
    other = 1 - tp
    toks, half = tok.shape
    width = 2 * half
    top = routes_ref.shape[0]
    chunks = half // LANES
    spread = rem * chunks
    paired = n & (n - 1) == 0
    parts = 2 if rem else 1

    def peer(d, sign):
        if not paired:
            return lax.rem(me + sign * d + n, n)
        where, bit = me, 1
        while bit < n:
            if d & bit:
                where = where + bit * (1 - 2 * lax.rem(me // bit, 2))
            bit *= 2
        return where

    target = [peer(d, 1) for d in seq]
    source = [peer(d, -1) for d in seq]

    barrier = pltpu.get_barrier_semaphore()
    for i in sends:
        pl.semaphore_signal(barrier, inc=1, device_id={"ep": target[i]}, device_id_type=MESH)
    pl.semaphore_signal(barrier, inc=1, device_id={"tp": other}, device_id_type=MESH)

    first = [
        pltpu.make_async_copy(routes_hbm, routes_ref, i_sem.at[0]),
        pltpu.make_async_copy(tokens_hbm, tok, i_sem.at[1]),
        pltpu.make_async_copy(logits_hbm, logits_ref, i_sem.at[2]),
        pltpu.make_async_copy(gain_hbm, affine.at[0, 0], i_sem.at[3]),
        pltpu.make_async_copy(shift_hbm, affine.at[0, 1], i_sem.at[4]),
    ]
    loads = []
    for j, side in enumerate((tp, other)):
        span = pl.ds(pl.multiple_of(side * half, half), half)
        loads += [
            pltpu.make_async_copy(wg_hbm.at[0, span], wg.at[j], w_sem.at[3 * j]),
            pltpu.make_async_copy(wu_hbm.at[0, span], wu.at[j], w_sem.at[3 * j + 1]),
            pltpu.make_async_copy(wd_hbm.at[0, :, span], wd.at[j], w_sem.at[3 * j + 2]),
        ]
    for load in first + loads:
        load.start()
    for load in first:
        load.wait()

    routes = routes_ref[...]
    logits = jnp.exp(logits_ref[...])
    weights = logits / jnp.sum(logits, axis=0, keepdims=True)
    before = jnp.where(iota((toks, toks), 0) < iota((toks, toks), 1), 1.0, 0.0).astype(bf16)

    def choose(place, rank):
        shape = place.shape
        expert = jnp.zeros(shape, jnp.int32)
        for i in range(n):
            expert = jnp.where(place == i, target[i], expert)
        named = jnp.zeros(shape, f32)
        share = jnp.zeros(shape, f32)
        for k in range(top):
            hit = routes[k:k + 1, :] == expert
            named = jnp.where(hit, 1.0, named)
            share = jnp.where(hit, weights[k:k + 1, :], share)
        chosen = (named > 0.5) & (dot(named.astype(bf16), before) == rank.astype(f32))
        return jnp.where(chosen, 1.0, 0.0), jnp.where(chosen, share, 0.0)

    def split(share):
        whole = jnp.transpose(share)
        a = whole.astype(bf16)
        rest = whole - a.astype(f32)
        b = rest.astype(bf16)
        return a, b, (rest - b.astype(f32)).astype(bf16)

    row = iota((n * base, toks), 0)
    pick, share = choose(row // base, row % base)
    outb1[...] = dot(pick.astype(bf16), tok[...]).astype(bf16).reshape(n, base, half)
    share_main = split(share)
    if rem:
        row = iota((n * spread, toks), 0)
        pick, _ = choose(row // spread, base + row % rem)
        chunk = row % spread // rem
        total = jnp.zeros((n * spread, LANES), f32)
        for c in range(chunks):
            total += dot(
                jnp.where(chunk == c, pick, 0.0).astype(bf16), tok[:, c * LANES:(c + 1) * LANES]
            )
        outb2[...] = total.astype(bf16).reshape(n, spread, LANES)
        row = iota((n * rem, toks), 0)
        _, share = choose(row // rem, base + row % rem)
        share_extra = split(share)

    def unpack(flat, count):
        size = count * spread
        r, z = iota((size, size), 0), iota((size, size), 1)
        c, q = r // (count * rem), r % (count * rem)
        where = q // rem * spread + c * rem + q % rem
        rows = dot(jnp.where(where == z, 1.0, 0.0).astype(bf16), flat)
        block = count * rem
        return jnp.concatenate([rows[c * block:(c + 1) * block] for c in range(chunks)], axis=1)

    def repack(rows, count):
        size = count * spread
        z, r = iota((size, size), 0), iota((size, size), 1)
        c, q = r // (count * rem), r % (count * rem)
        where = q // rem * spread + c * rem + q % rem
        flat = jnp.concatenate(
            [rows[:, c * LANES:(c + 1) * LANES] for c in range(chunks)], axis=0
        ).astype(bf16)
        return dot(jnp.where(where == z, 1.0, 0.0).astype(bf16), flat).astype(bf16)

    def across(src, dst, i, part, send, recv, place):
        return pltpu.make_async_remote_copy(
            src, dst, send.at[2 * i + part], recv.at[2 * i + part], device_id=place,
            device_id_type=MESH,
        )

    def dispatch(i):
        place = {"ep": target[i]}
        pieces = [(outb1, rows1), (outb2, rows2)][:parts]
        return [
            across(a.at[i], b.at[0, i], i, p, d_send, d_recv, place)
            for p, (a, b) in enumerate(pieces)
        ]

    def forward(i):
        place = {"tp": other}
        pieces = [(outb1, rows1), (outb2, rows2)][:parts]
        return [
            across(b.at[0, i] if i else a.at[i], b.at[1, i], i, p, f_send, f_recv, place)
            for p, (a, b) in enumerate(pieces)
        ]

    def give_back(i):
        place = {"ep": source[i]}
        pieces = [(ans1, back1), (ans2, back2)][:parts]
        return [
            across(a.at[i], b.at[i], i, p, r_send, r_recv, place)
            for p, (a, b) in enumerate(pieces)
        ]

    def partial(g):
        return pltpu.make_async_remote_copy(
            part_out.at[g], part_in.at[g], p_send.at[g], p_recv.at[g], device_id={"tp": other},
            device_id_type=MESH,
        )

    affine_copy = pltpu.make_async_remote_copy(
        affine.at[0], affine.at[1], a_sem.at[0], a_sem.at[1], device_id={"tp": other},
        device_id_type=MESH,
    )

    pl.semaphore_wait(barrier, n)
    for i in sends:
        for copy in dispatch(i):
            copy.start()
    for copy in forward(0):
        copy.start()
    affine_copy.start()
    rows1[0, 0] = outb1[0]
    if rem:
        rows2[0, 0] = outb2[0]
    for load in loads:
        load.wait()
    affine_copy.wait_recv()

    def landed(g):
        lower, upper = groups[g]
        for i in [i for i in [0] + sends if lower <= i < upper and i]:
            for arrived, onward in zip(dispatch(i), forward(i)):
                arrived.wait_recv()
                onward.start()

    def gathered(j, lower, upper):
        count = upper - lower
        main = rows1[j, lower:upper].reshape(count * base, half).astype(f32)
        if not rem:
            return main
        extra = unpack(rows2[j, lower:upper].reshape(count * spread, LANES), count)
        return jnp.concatenate([main, extra], axis=0)

    def experts(g):
        lower, upper = groups[g]
        for i in range(lower, upper):
            for copy in forward(i):
                copy.wait_recv()
        x = [gathered(j, lower, upper) for j in range(2)]
        average = (
            jnp.sum(x[0], axis=1, keepdims=True) + jnp.sum(x[1], axis=1, keepdims=True)
        ) / width
        squares = (
            jnp.sum(x[0] * x[0], axis=1, keepdims=True)
            + jnp.sum(x[1] * x[1], axis=1, keepdims=True)
        ) / width
        scale = lax.rsqrt(squares - average * average + norm_eps)
        normed = [
            ((x[j] - average) * scale * affine[j, 0] + affine[j, 1]).astype(bf16)
            for j in range(2)
        ]
        gate = dot(normed[0], wg[0]) + dot(normed[1], wg[1])
        up = dot(normed[0], wu[0]) + dot(normed[1], wu[1])
        cut = jnp.minimum(gate, clamp_limit)
        hidden = (
            (jnp.clip(up, -clamp_limit, clamp_limit) + 1.0)
            * cut * jax.nn.sigmoid(sigmoid_slope * cut)
        ).astype(bf16)
        part_out[g] = dot(hidden, wd[1]).astype(bf16)
        partial(g).start()
        return dot(hidden, wd[0]).astype(bf16)

    def answer(g, mine):
        lower, upper = groups[g]
        count = upper - lower
        partial(g).wait_recv()
        total = (mine.astype(f32) + part_in[g].astype(f32)).astype(bf16)
        ans1[lower:upper] = total[:count * base].reshape(count, base, half)
        if rem:
            ans2[lower:upper] = repack(total[count * base:].astype(f32), count).reshape(
                count, spread, LANES
            )
        if lower == 0:
            back1[0] = ans1[0]
            if rem:
                back2[0] = ans2[0]
        for i in sends:
            if lower <= i < upper:
                for copy in give_back(i):
                    copy.start()

    for g in range(len(groups)):
        landed(g)
        answer(g, experts(g))
    for i in sends:
        for copy in give_back(i):
            copy.wait_recv()
    got = back1[...].reshape(n * base, half)
    mixed = dot(share_main[2], got) + dot(share_main[1], got) + dot(share_main[0], got)
    if rem:
        got = unpack(back2[...].reshape(n * spread, LANES), n).astype(bf16)
        mixed += dot(share_extra[2], got) + dot(share_extra[1], got) + dot(share_extra[0], got)
    out_ref[...] = mixed.astype(bf16)
    affine_copy.wait_send()
    for g in range(len(groups)):
        partial(g).wait_send()
    for i in range(n):
        for copy in forward(i) + (dispatch(i) + give_back(i) if i else []):
            copy.wait_send()


def body(tokens, routes, gate_logits, norm_gain, norm_shift, gate_weight, up_weight, down_weight):
    n = lax.axis_size("ep")
    toks, top = routes.shape
    half = tokens.shape[1]
    cap = toks * top // n + 2
    base, rem = cap // 8 * 8, cap % 8
    if base == 0 or rem > 4:
        base, rem = -(-cap // 8) * 8, 0
    ff = gate_weight.shape[2]
    if n % 4 == 0:
        q = n // 4
        seq = [*range(q), *range(2 * q, 3 * q), *range(3 * q, n), *range(q, 2 * q)]
        groups = [(0, 2 * q), (2 * q, n)]
        sends = [*range(q, 2 * q), *range(1, q), *range(2 * q, n)]
    else:
        seq, groups, sends = list(range(n)), [(0, n)], list(range(n - 1, 0, -1))
    count = groups[0][1]
    spread = max(rem, 1) * half // 128
    anywhere = pl.BlockSpec(memory_space=pl.ANY)
    main = pltpu.VMEM((n, base, half), bf16)
    extra = pltpu.VMEM((n, spread, 128), bf16)
    exchange = pltpu.VMEM((len(groups), count * (base + rem), half), bf16)
    dma = pltpu.SemaphoreType.DMA
    sems = dma((2 * n,))
    return pl.pallas_call(
        functools.partial(kernel, n, base, rem, seq, groups, sends),
        out_shape=jax.ShapeDtypeStruct((toks, half), bf16),
        in_specs=[anywhere] * 8,
        out_specs=pl.BlockSpec(memory_space=pltpu.VMEM),
        scratch_shapes=[
            pltpu.VMEM((toks, half), bf16),
            pltpu.VMEM((top, toks), jnp.int32),
            pltpu.VMEM((top, toks), f32),
            pltpu.VMEM((2, 2, 1, half), f32),
            pltpu.VMEM((2, half, ff), bf16),
            pltpu.VMEM((2, half, ff), bf16),
            pltpu.VMEM((2, ff, half), bf16),
            main, extra,
            pltpu.VMEM((2, n, base, half), bf16),
            pltpu.VMEM((2, n, spread, 128), bf16),
            exchange, exchange,
            main, extra, main, extra,
            dma((5,)), dma((6,)), dma((2,)),
            sems, sems, sems, sems, dma((len(groups),)), dma((len(groups),)), sems, sems,
        ],
        compiler_params=pltpu.CompilerParams(collective_id=0, has_side_effects=True),
    )(
        tokens, routes.T, gate_logits.T, norm_gain.reshape(1, half), norm_shift.reshape(1, half),
        gate_weight, up_weight, down_weight,
    )


def solution(mesh):
    placed = (
        P(("grp", "ep"), "tp"),
        P(("grp", "ep"), None),
        P(("grp", "ep"), None),
        P("tp"),
        P("tp"),
        P("ep", None, "tp"),
        P("ep", None, "tp"),
        P("ep", "tp", None),
    )
    return jax.shard_map(
        body, mesh=mesh, in_specs=placed, out_specs=P(("grp", "ep"), "tp"), check_vma=False
    )
```

time: 77.1 us -> 29.5 us (0.38)
  Pallas kernels: 0 us -> 27.9 us
  blocking collectives: 23.9 us -> 0 us
  waiting for transfers between devices: 19.1 us -> 0 us
  between operations: 13.5 us -> 0.01 us
  starting transfers between devices: 5.72 us -> 0 us
  matrix products: 5.3 us -> 0 us
  local copies, waits for them, and re-layouts: 5.87 us -> 1.47 us
  other arithmetic: 3.3 us -> 0 us
    pallas_call x0 -> x1, Pallas kernels: none -> 27.9 us  [body(): pl.pallas_call(functools.partial(kernel, n, base, rem, seq, groups, sends...]
    all_to_all x1 -> x0, blocking collectives: 19.3 us -> none  [body(): lax.all_to_all(outgoing.reshape(ep_count, capacity, send_width), 'ep', sp...]
    all_to_all x1 -> x0, waiting for transfers between devices: 12 us -> none  [body(): lax.all_to_all(answered, 'ep', split_axis=0, concat_axis=0, tiled=True)]
    reduce_scatter x1 -> x0, waiting for transfers between devices: 7 us -> none  [expert_apply(): lax.psum_scatter(partial_out.reshape(sources, slots_here, width), 'tp', s...]
    all_to_all x1 -> x0, starting transfers between devices: 5.72 us -> none  [body(): lax.all_to_all(answered, 'ep', split_axis=0, concat_axis=0, tiled=True)]
    dot_general x2 -> x0, matrix products: 5.3 us -> none  [the longest x1 2.78 us: expert_apply(): jnp.dot(row_block, gate_weight[0], preferred_element_type=jnp.float32)]
    all_gather x2 -> x0, blocking collectives: 4.61 us -> none  [the longest x1 2.36 us: expert_apply(): whole = lax.all_gather(received, 'tp', axis=2, tiled=True)]
    scatter x1 -> x0, local copies, waits for them, and re-layouts: 2.11 us -> none  [body(): outgoing = jnp.zeros((ep_count * capacity, send_width), jnp.bfloat16).at[...]
  transfers between devices with their start and end apart: 2 -> 0, of which waited for: 2 -> 0; matrix products, arithmetic and copies ran while one was open for 0% -> 0% of each run, Pallas kernels for 0% -> 0%
where the time goes in v2:
time: 29.5 us; the launch traced here: 29.4 us
  Pallas kernels  27.9 us (95%)
  local copies, waits for them, and re-layouts  1.47 us (5%)
    pallas_call x1, Pallas kernels, body(): pl.pallas_call(functools.partial(kernel, n, base, rem, seq, groups, sends...  27.9 us
    unnamed x1, local copies, waits for them, and re-layouts  1.47 us

profile of v2, /device:TPU:0, one launch (start us, length us, event | category | flops | bytes accessed | tf_op | source)
XLA Modules:
  0.0 29.4 jit_solution(4530697716471415238)
XLA Ops:
  0.0 27.9 %shard_map.82 = bf16[32,1024]{1,0:T(8,128)(2,1)} custom-call(bf16[32,1024]{1,0:T(8,128)(2,1)} %tokens_hbm.1, s32[4,32]{1,0:T(4,128)} %bitcast.6, f32[4,32]{1,0:T(4,128)} %bitcast.7, f32[1,1024]{1,0:T(1,128)} %bitcast.4, f32[1,1024]{1,0:T(1,128)} %bitcast.5, bf16[1,2048,512]{2,1,0:T(8,128)(2,1)} %wg_hbm.1, bf16[1,2048,512]{2,1,0:T(8,128)(2,1)} %wu_hbm.1, ...), custom_call_target="tpu_custom_call" | custom-call | tf_op jit(solution)/shard_map/pallas_call | solution.py:309
  27.9 1.5 %copy.10 = bf16[32,1024]{1,0:T(8,128)(2,1)} copy(bf16[32,1024]{1,0:T(8,128)(2,1)} %shard_map.82) | data formatting | bytes 131072

commit v3 on v2

--- a/solution.py
+++ b/solution.py
@@ -30,7 +30,7 @@
     out_ref,
     tok, routes_ref, logits_ref, affine, wg, wu, wd,
     outb1, outb2, rows1, rows2, part_out, part_in, ans1, ans2, back1, back2,
-    i_sem, w_sem, a_sem, d_send, d_recv, f_send, f_recv, p_send, p_recv, r_send, r_recv,
+    i_sem, w_sem, a_sem, d_send, d_recv, f_send, f_recv, p_send, p_recv, r_send, r_recv, ready,
 ):
     me = lax.axis_index("ep")
     tp = lax.axis_index("tp")
@@ -57,7 +57,9 @@
     source = [peer(d, -1) for d in seq]
 
     barrier = pltpu.get_barrier_semaphore()
-    for i in sends:
+    staged = paired and n >= 4
+    greeted = [i for i in sends if seq[i] <= n // 2] if staged else sends
+    for i in greeted:
         pl.semaphore_signal(barrier, inc=1, device_id={"ep": target[i]}, device_id_type=MESH)
     pl.semaphore_signal(barrier, inc=1, device_id={"tp": other}, device_id_type=MESH)
 
@@ -185,13 +187,24 @@
         device_id_type=MESH,
     )
 
-    pl.semaphore_wait(barrier, n)
+    pl.semaphore_wait(barrier, len(greeted) + 1)
+    if staged:
+        for i in greeted:
+            if seq[i] < n // 2:
+                pl.semaphore_signal(
+                    ready.at[seq[i]], inc=1, device_id={"ep": target[i]}, device_id_type=MESH
+                )
+    started = 0
     for i in sends:
+        if staged and seq[i] > n // 2:
+            pl.semaphore_wait(ready.at[seq[i] - n // 2], 1)
         for copy in dispatch(i):
             copy.start()
-    for copy in forward(0):
-        copy.start()
-    affine_copy.start()
+        if not started:
+            for copy in forward(0):
+                copy.start()
+            affine_copy.start()
+            started = 1
     rows1[0, 0] = outb1[0]
     if rem:
         rows2[0, 0] = outb2[0]
@@ -262,9 +275,12 @@
                 for copy in give_back(i):
                     copy.start()
 
+    landed(0)
     for g in range(len(groups)):
-        landed(g)
-        answer(g, experts(g))
+        mine = experts(g)
+        if g + 1 < len(groups):
+            landed(g + 1)
+        answer(g, mine)
     for i in sends:
         for copy in give_back(i):
             copy.wait_recv()
@@ -295,7 +311,7 @@
         q = n // 4
         seq = [*range(q), *range(2 * q, 3 * q), *range(3 * q, n), *range(q, 2 * q)]
         groups = [(0, 2 * q), (2 * q, n)]
-        sends = [*range(q, 2 * q), *range(1, q), *range(2 * q, n)]
+        sends = [q, *range(1, q), *range(q + 1, 2 * q), *range(2 * q, n)]
     else:
         seq, groups, sends = list(range(n)), [(0, n)], list(range(n - 1, 0, -1))
     count = groups[0][1]
@@ -308,7 +324,7 @@
     sems = dma((2 * n,))
     return pl.pallas_call(
         functools.partial(kernel, n, base, rem, seq, groups, sends),
-        out_shape=jax.ShapeDtypeStruct((toks, half), bf16),
+        out_shape=pltpu.VMEM((toks, half), bf16),
         in_specs=[anywhere] * 8,
         out_specs=pl.BlockSpec(memory_space=pltpu.VMEM),
         scratch_shapes=[
@@ -326,6 +342,7 @@
             main, extra, main, extra,
             dma((5,)), dma((6,)), dma((2,)),
             sems, sems, sems, sems, dma((len(groups),)), dma((len(groups),)), sems, sems,
+            pltpu.SemaphoreType.REGULAR((n,)),
         ],
         compiler_params=pltpu.CompilerParams(collective_id=0, has_side_effects=True),
     )(

time: 29.5 us -> 26.2 us (0.89)
  Pallas kernels: 27.9 us -> 25.4 us
  local copies, waits for them, and re-layouts: 1.47 us -> 0.63 us
    pallas_call x1, Pallas kernels: 27.9 us -> 25.4 us  [body(): pl.pallas_call(functools.partial(kernel, n, base, rem, seq, groups, sends...]
    unnamed x1, local copies, waits for them, and re-layouts: 1.47 us -> 0.63 us
where the time goes in v3:
time: 26.2 us; the launch traced here: 26.1 us
  Pallas kernels  25.4 us (97%)
  local copies, waits for them, and re-layouts  0.63 us (2%)
    pallas_call x1, Pallas kernels, body(): pl.pallas_call(functools.partial(kernel, n, base, rem, seq, groups, sends...  25.4 us
    unnamed x1, local copies, waits for them, and re-layouts  0.63 us

profile of v3, /device:TPU:0, one launch (start us, length us, event | category | flops | bytes accessed | tf_op | source)
XLA Modules:
  0.0 26.1 jit_solution(12650011578096594448)
XLA Ops:
  0.0 25.4 %shard_map.82 = bf16[32,1024]{1,0:T(8,128)(2,1)S(1)} custom-call(bf16[32,1024]{1,0:T(8,128)(2,1)} %tokens_hbm.1, s32[4,32]{1,0:T(4,128)} %bitcast.6, f32[4,32]{1,0:T(4,128)} %bitcast.7, f32[1,1024]{1,0:T(1,128)} %bitcast.4, f32[1,1024]{1,0:T(1,128)} %bitcast.5, bf16[1,2048,512]{2,1,0:T(8,128)(2,1)} %wg_hbm.1, bf16[1,2048,512]{2,1,0:T(8,128)(2,1)} %wu_hbm.1, ...), custom_call_target="tpu_custom_call" | custom-call | tf_op jit(solution)/shard_map/pallas_call | solution.py:325
  25.4 0.6 %copy.10 = bf16[32,1024]{1,0:T(8,128)(2,1)} copy(bf16[32,1024]{1,0:T(8,128)(2,1)S(1)} %shard_map.82) | data formatting | bytes 131072

commit v4 on v3

--- a/solution.py
+++ b/solution.py
@@ -53,6 +53,7 @@
             bit *= 2
         return where
 
+    sizes = [((b - a) * (base + rem), -(-(b - a) * (base + rem) // 8) * 8) for a, b in groups]
     target = [peer(d, 1) for d in seq]
     source = [peer(d, -1) for d in seq]
 
@@ -112,7 +113,7 @@
     row = iota((n * base, toks), 0)
     pick, share = choose(row // base, row % base)
     outb1[...] = dot(pick.astype(bf16), tok[...]).astype(bf16).reshape(n, base, half)
-    share_main = split(share)
+    share_main = [split(share[lower * base:upper * base]) for lower, upper in groups]
     if rem:
         row = iota((n * spread, toks), 0)
         pick, _ = choose(row // spread, base + row % rem)
@@ -125,7 +126,7 @@
         outb2[...] = total.astype(bf16).reshape(n, spread, LANES)
         row = iota((n * rem, toks), 0)
         _, share = choose(row // rem, base + row % rem)
-        share_extra = split(share)
+        share_extra = [split(share[lower * rem:upper * rem]) for lower, upper in groups]
 
     def unpack(flat, count):
         size = count * spread
@@ -178,7 +179,7 @@
 
     def partial(g):
         return pltpu.make_async_remote_copy(
-            part_out.at[g], part_in.at[g], p_send.at[g], p_recv.at[g], device_id={"tp": other},
+            part_out.at[g, pl.ds(0, sizes[g][1])], part_in.at[g, pl.ds(0, sizes[g][1])], p_send.at[g], p_recv.at[g], device_id={"tp": other},
             device_id_type=MESH,
         )
 
@@ -252,7 +253,7 @@
             (jnp.clip(up, -clamp_limit, clamp_limit) + 1.0)
             * cut * jax.nn.sigmoid(sigmoid_slope * cut)
         ).astype(bf16)
-        part_out[g] = dot(hidden, wd[1]).astype(bf16)
+        part_out[g, :sizes[g][0]] = dot(hidden, wd[1]).astype(bf16)
         partial(g).start()
         return dot(hidden, wd[0]).astype(bf16)
 
@@ -260,8 +261,11 @@
         lower, upper = groups[g]
         count = upper - lower
         partial(g).wait_recv()
-        total = (mine.astype(f32) + part_in[g].astype(f32)).astype(bf16)
+        total = (mine.astype(f32) + part_in[g, :sizes[g][0]].astype(f32)).astype(bf16)
         ans1[lower:upper] = total[:count * base].reshape(count, base, half)
+        for i in sends:
+            if lower <= i < upper:
+                give_back(i)[0].start()
         if rem:
             ans2[lower:upper] = repack(total[count * base:].astype(f32), count).reshape(
                 count, spread, LANES
@@ -272,7 +276,7 @@
                 back2[0] = ans2[0]
         for i in sends:
             if lower <= i < upper:
-                for copy in give_back(i):
+                for copy in give_back(i)[1:]:
                     copy.start()
 
     landed(0)
@@ -281,14 +285,20 @@
         if g + 1 < len(groups):
             landed(g + 1)
         answer(g, mine)
-    for i in sends:
-        for copy in give_back(i):
-            copy.wait_recv()
-    got = back1[...].reshape(n * base, half)
-    mixed = dot(share_main[2], got) + dot(share_main[1], got) + dot(share_main[0], got)
-    if rem:
-        got = unpack(back2[...].reshape(n * spread, LANES), n).astype(bf16)
-        mixed += dot(share_extra[2], got) + dot(share_extra[1], got) + dot(share_extra[0], got)
+    mixed = jnp.zeros((toks, half), f32)
+    for g, (lower, upper) in enumerate(groups):
+        for i in sends:
+            if lower <= i < upper:
+                for copy in give_back(i):
+                    copy.wait_recv()
+        count = upper - lower
+        got = back1[lower:upper].reshape(count * base, half)
+        for piece in reversed(share_main[g]):
+            mixed += dot(piece, got)
+        if rem:
+            got = unpack(back2[lower:upper].reshape(count * spread, LANES), count).astype(bf16)
+            for piece in reversed(share_extra[g]):
+                mixed += dot(piece, got)
     out_ref[...] = mixed.astype(bf16)
     affine_copy.wait_send()
     for g in range(len(groups)):
@@ -309,8 +319,8 @@
     ff = gate_weight.shape[2]
     if n % 4 == 0:
         q = n // 4
-        seq = [*range(q), *range(2 * q, 3 * q), *range(3 * q, n), *range(q, 2 * q)]
-        groups = [(0, 2 * q), (2 * q, n)]
+        seq = [*range(q), *range(2 * q, 3 * q), *range(q, 2 * q), *range(3 * q, n)]
+        groups = [(0, 3 * q), (3 * q, n)]
         sends = [q, *range(1, q), *range(q + 1, 2 * q), *range(2 * q, n)]
     else:
         seq, groups, sends = list(range(n)), [(0, n)], list(range(n - 1, 0, -1))
@@ -319,7 +329,7 @@
     anywhere = pl.BlockSpec(memory_space=pl.ANY)
     main = pltpu.VMEM((n, base, half), bf16)
     extra = pltpu.VMEM((n, spread, 128), bf16)
-    exchange = pltpu.VMEM((len(groups), count * (base + rem), half), bf16)
+    exchange = pltpu.VMEM((len(groups), -(-count * (base + rem) // 8) * 8, half), bf16)
     dma = pltpu.SemaphoreType.DMA
     sems = dma((2 * n,))
     return pl.pallas_call(

time: 26.2 us -> 25.9 us (0.989)
  Pallas kernels: 25.4 us -> 25.1 us
    pallas_call x1, Pallas kernels: 25.4 us -> 25.1 us  [body(): pl.pallas_call(functools.partial(kernel, n, base, rem, seq, groups, sends...]
where the time goes in v4:
time: 25.9 us; the launch traced here: 25.7 us
  Pallas kernels  25.1 us (97%)
  local copies, waits for them, and re-layouts  0.63 us (2%)
    pallas_call x1, Pallas kernels, body(): pl.pallas_call(functools.partial(kernel, n, base, rem, seq, groups, sends...  25.1 us
    unnamed x1, local copies, waits for them, and re-layouts  0.63 us

profile of v4, /device:TPU:0, one launch (start us, length us, event | category | flops | bytes accessed | tf_op | source)
XLA Modules:
  0.0 25.7 jit_solution(13587377809723090056)
XLA Ops:
  0.0 25.1 %shard_map.82 = bf16[32,1024]{1,0:T(8,128)(2,1)S(1)} custom-call(bf16[32,1024]{1,0:T(8,128)(2,1)} %tokens_hbm.1, s32[4,32]{1,0:T(4,128)} %bitcast.6, f32[4,32]{1,0:T(4,128)} %bitcast.7, f32[1,1024]{1,0:T(1,128)} %bitcast.4, f32[1,1024]{1,0:T(1,128)} %bitcast.5, bf16[1,2048,512]{2,1,0:T(8,128)(2,1)} %wg_hbm.1, bf16[1,2048,512]{2,1,0:T(8,128)(2,1)} %wu_hbm.1, ...), custom_call_target="tpu_custom_call" | custom-call | tf_op jit(solution)/shard_map/pallas_call | solution.py:335
  25.1 0.6 %copy.10 = bf16[32,1024]{1,0:T(8,128)(2,1)} copy(bf16[32,1024]{1,0:T(8,128)(2,1)S(1)} %shard_map.82) | data formatting | bytes 131072
